TPU v7x, 32 devices: a whole 2x2x4 slice. The times are simulated.
32 devices in a mesh: grp: 2 (over x), ep: 16 (over z, y, core).
Axes of the slice: x: 2, y: 2, z: 4, core: 2. Of those that a mesh axis runs over, the one named last changes fastest.
Arguments:
- residual: bfloat16 [16, 4096], P('grp', 'ep'), parts along dimension 0, may hold values from -6 to 6
- head_states: float32 [64, 512, 1024], P(('grp', 'ep')), parts along dimension 0, may hold values from -6 to 6
- first_gain: bfloat16 [4096], replicated, may hold values from 0.099609375 to 1.8984375
- w_query: bfloat16 [4096, 2048], P(None, 'ep'), may hold values from -0.09375 to 0.09375
- w_key: bfloat16 [4096, 2048], P(None, 'ep'), may hold values from -0.09375 to 0.09375
- w_value: bfloat16 [4096, 4096], P(None, 'ep'), may hold values from -0.09375 to 0.09375
- w_gate: bfloat16 [4096, 4096], P(None, 'ep'), may hold values from -0.09375 to 0.09375
- w_low: bfloat16 [4096, 16], replicated, may hold values from -0.09375 to 0.09375
- w_decay: bfloat16 [16, 2048], replicated, may hold values from -15 to 15
- decay_bias: float32 [2048], replicated, may hold values from -40 to 4
- head_gain: bfloat16 [1024], replicated, may hold values from 0.099609375 to 1.8984375
- w_output: bfloat16 [4096, 4096], P(None, 'ep'), may hold values from -0.09375 to 0.09375
- second_gain: bfloat16 [4096], replicated, may hold values from 0.099609375 to 1.8984375
- routes: int32 [16, 2], P('grp'), parts along dimension 0, may hold values from 0 to 15, as said below
- group_logits: float32 [16, 4], P('grp'), parts along dimension 0, may hold values from -12 to 12
- expert_logits: float32 [16, 2], P('grp'), parts along dimension 0, may hold values from -9 to 9
- expert_gate: bfloat16 [16, 4096, 512], P('ep'), may hold values from -0.09375 to 0.09375
- expert_up: bfloat16 [16, 4096, 512], P('ep'), may hold values from -0.09375 to 0.09375
- expert_down: bfloat16 [16, 512, 4096], P('ep'), may hold values from -0.25 to 0.25
Outputs:
- layer_out: bfloat16 [16, 4096], P('grp', 'ep'), parts along dimension 0
- new_states: float32 [64, 512, 1024], P(('grp', 'ep')), parts along dimension 0
There are 2 independent parts, one for each index of `grp`. A program takes and returns all parts, laid end to end along the dimension named above; an argument that names none is the same for every part. Nothing has to cross between parts.
Inputs may be any that keep to these rules, and one draw needn't show every extreme that they name: `routes`: each row names 2 different experts of one group (numbers g * 4 to g * 4 + 3). No expert is named by more than 2 rows, and in every draw all experts of one group are named by exactly 2 rows.
All inputs are finite; a program needn't handle non-finite values.
Results may differ from a plain program's by a relative error of at most 0.014.
Values may be sent and summed in bfloat16 or wider, within the bound.
No kernel may reach another device: no remote copies, remote signals or barrier semaphores. Data moves between devices by JAX's collectives and lax.ppermute only.
A program may use at most 128 MiB of HBM per device.

v0:
```python
import jax
import jax.numpy as jnp
import numpy as np
from jax import lax
from jax.sharding import PartitionSpec as P

HEADS = 4
DK = 512
DV = 1024
GROUPS = 4
TOP = 2
norm_eps = 1e-06
decay_tau = 16.0


def rms_scale(values, gain):
    floats = values.astype(jnp.float32)
    return (
        floats
        * lax.rsqrt(jnp.mean(floats * floats, axis=-1, keepdims=True) + norm_eps)
        * gain.astype(jnp.float32)
    )


def route_weights(routes, group_logits, expert_logits, per_group):
    group_exp = jnp.exp(group_logits)
    group_prob = group_exp / jnp.sum(group_exp, axis=1, keepdims=True)
    chosen = routes[:, 0] // per_group
    groups_row = jnp.arange(group_logits.shape[1], dtype=jnp.int32)
    picked = jnp.sum(
        group_prob * (chosen[:, None] == groups_row[None, :]).astype(jnp.float32), axis=1
    )
    expert_exp = jnp.exp(expert_logits)
    return expert_exp / jnp.sum(expert_exp, axis=1, keepdims=True) * picked[:, None]


def per_device(
    residual,
    head_states,
    first_gain,
    w_query,
    w_key,
    w_value,
    w_gate,
    w_low,
    w_decay,
    decay_bias,
    head_gain,
    w_output,
    second_gain,
    routes,
    group_logits,
    expert_logits,
    expert_gate,
    expert_up,
    expert_down,
):
    devices = lax.axis_size("ep")
    my_index = lax.axis_index("ep")
    seq_count = residual.shape[0]
    own_width = residual.shape[1]
    width = own_width * devices
    pairs_dev = head_states.shape[0]
    slot_count = max(1, pairs_dev // HEADS)
    rows = lax.all_gather(residual, "ep", axis=1, tiled=True)
    normed = rms_scale(rows, first_gain).astype(jnp.bfloat16)
    my_head = my_index * HEADS // devices
    target = jnp.arange(devices, dtype=jnp.int32)[:, None]
    turn = jnp.arange(slot_count, dtype=jnp.int32)[None, :]
    within = jnp.mod(my_head - target * pairs_dev, HEADS) + turn * HEADS
    target_seq = (target * pairs_dev + within) // HEADS
    seq_row = jnp.arange(seq_count, dtype=jnp.int32)[None, None, :]
    picker = (target_seq[:, :, None] == seq_row) & (within < pairs_dev)[:, :, None]
    picker = picker.astype(jnp.bfloat16).reshape(devices * slot_count, seq_count)

    def outgoing(weight):
        projected = jnp.dot(normed, weight, preferred_element_type=jnp.float32).astype(jnp.bfloat16)
        placed = jnp.dot(picker, projected, preferred_element_type=jnp.float32).astype(jnp.bfloat16)
        return placed.reshape(devices, slot_count, projected.shape[1])

    send_query = outgoing(w_query)
    send_key = outgoing(w_key)
    send_value = outgoing(w_value)
    send_gate = outgoing(w_gate)
    incoming = (
        lax.all_to_all(send_query, "ep", split_axis=0, concat_axis=0, tiled=True),
        lax.all_to_all(send_key, "ep", split_axis=0, concat_axis=0, tiled=True),
        lax.all_to_all(send_value, "ep", split_axis=0, concat_axis=0, tiled=True),
        lax.all_to_all(send_gate, "ep", split_axis=0, concat_axis=0, tiled=True),
    )
    pair_ids = my_index * pairs_dev + jnp.arange(pairs_dev, dtype=jnp.int32)
    head_pick = (
        jnp.mod(pair_ids, HEADS)[:, None] == jnp.arange(HEADS, dtype=jnp.int32)[None, :]
    ).astype(jnp.bfloat16)
    turns = np.arange(pairs_dev) // HEADS
    pair_rows = np.arange(pairs_dev)

    def arrange(received):
        merged = jnp.dot(head_pick, received.reshape(HEADS, -1), preferred_element_type=jnp.float32)
        merged = merged.reshape(pairs_dev, devices // HEADS, slot_count, received.shape[2])
        return merged[pair_rows, :, turns, :].reshape(pairs_dev, -1).astype(jnp.bfloat16)

    query = arrange(incoming[0])
    key = arrange(incoming[1])
    value = arrange(incoming[2])
    gate = arrange(incoming[3])
    low = jnp.dot(normed, w_low, preferred_element_type=jnp.float32)
    decay_pre = (
        jnp.dot(low, w_decay.astype(jnp.float32), precision=lax.Precision.HIGHEST) + decay_bias
    )
    decay_pre = lax.dynamic_slice_in_dim(
        decay_pre.reshape(seq_count * HEADS, DK), my_index * pairs_dev, pairs_dev, 0
    )
    log_decay = jax.nn.log_sigmoid(decay_pre) / decay_tau
    new_states = (
        head_states * jnp.exp(log_decay)[:, :, None]
        + key.astype(jnp.float32)[:, :, None] * value.astype(jnp.float32)[:, None, :]
    )
    read = jnp.einsum(
        "pk,pkv->pv",
        query.astype(jnp.float32) * DK ** (-0.5),
        new_states,
        precision=lax.Precision.HIGHEST,
    )
    mixed = (rms_scale(read, head_gain) * jax.nn.silu(gate.astype(jnp.float32))).astype(
        jnp.bfloat16
    )
    gathered = lax.all_gather(mixed, "ep", axis=0, tiled=True).reshape(seq_count, HEADS * DV)
    branch = jnp.dot(gathered, w_output, preferred_element_type=jnp.float32).astype(jnp.bfloat16)
    stream = (residual.astype(jnp.float32) + branch.astype(jnp.float32)).astype(jnp.bfloat16)
    floats = stream.astype(jnp.float32)
    total = lax.psum(jnp.sum(floats * floats, axis=1), "ep")
    gain_part = lax.dynamic_slice_in_dim(second_gain, my_index * own_width, own_width)
    scaled = floats * lax.rsqrt(total / width + norm_eps)[:, None] * gain_part.astype(jnp.float32)
    expert_in = lax.all_gather(scaled.astype(jnp.bfloat16), "ep", axis=1, tiled=True)
    capacity = 2 * seq_count * TOP // devices
    weights = route_weights(routes, group_logits, expert_logits, devices // GROUPS)
    hits = (routes == my_index).astype(jnp.int32)
    mine = jnp.sum(weights * hits.astype(jnp.float32), axis=1)
    routed = jnp.sum(hits, axis=1)
    slot = jnp.cumsum(routed) - routed
    chooser = (slot[None, :] == jnp.arange(capacity, dtype=jnp.int32)[:, None]) & (
        routed[None, :] > 0
    )
    picked = jnp.dot(
        chooser.astype(jnp.bfloat16), expert_in, preferred_element_type=jnp.float32
    ).astype(jnp.bfloat16)
    row_weight = jnp.dot(chooser.astype(jnp.float32), mine, precision=lax.Precision.HIGHEST)
    gate_part = jnp.dot(picked, expert_gate[0], preferred_element_type=jnp.float32)
    up_part = jnp.dot(picked, expert_up[0], preferred_element_type=jnp.float32)
    active = (jax.nn.silu(gate_part) * up_part * row_weight[:, None]).astype(jnp.bfloat16)
    expert_rows = jnp.dot(active, expert_down[0], preferred_element_type=jnp.float32).astype(
        jnp.bfloat16
    )
    arrived = lax.all_to_all(expert_rows, "ep", split_axis=1, concat_axis=0, tiled=True)
    every = jnp.arange(devices, dtype=jnp.int32)
    hit_all = jnp.sum((routes[:, :, None] == every[None, None, :]).astype(jnp.int32), axis=1)
    slot_all = jnp.cumsum(hit_all, axis=0) - hit_all
    placer = (slot_all[:, :, None] == jnp.arange(capacity, dtype=jnp.int32)[None, None, :]) & (
        hit_all[:, :, None] > 0
    )
    placer = placer.astype(jnp.bfloat16).reshape(seq_count, devices * capacity)
    returned = jnp.dot(placer, arrived, preferred_element_type=jnp.float32)
    layer_out = (stream.astype(jnp.float32) + returned).astype(jnp.bfloat16)
    return (layer_out, new_states)


def solution(mesh):
    return jax.shard_map(
        per_device,
        mesh=mesh,
        in_specs=(
            P("grp", "ep"),
            P(("grp", "ep"), None, None),
            P(),
            P(None, "ep"),
            P(None, "ep"),
            P(None, "ep"),
            P(None, "ep"),
            P(),
            P(),
            P(),
            P(),
            P(None, "ep"),
            P(),
            P("grp", None),
            P("grp", None),
            P("grp", None),
            P("ep", None, None),
            P("ep", None, None),
            P("ep", None, None),
        ),
        out_specs=(P("grp", "ep"), P(("grp", "ep"), None, None)),
        check_vma=False,
    )
```

profile of v0, /device:TPU:0, one launch (start us, length us, event | category | flops | bytes accessed | tf_op | source)
XLA Modules:
  0.0 169.2 jit_solution(12246803465482614124)
XLA Ops:
  0.7 23.7 %all_gather.9 = bf16[8,4096]{1,0:T(8,128)(2,1)S(1)} all-gather(bf16[8,256]{1,0:T(8,128)(2,1)} %param.29), channel_id=1, replica_groups=mesh['grp'=2,'ep'=16] {'ep'}, dimensions={1}, use_global_device_ids=true | all-gather | bytes 69632 | tf_op jit(solution)/shard_map/all_gather | solution.py:65
  24.6 0.7 convert_element_type.145
  25.3 1.6 fusion.14
  26.9 0.6 copy.61
  27.5 3.4 %all-to-all-start.1 = ((bf16[16,1,128]{2,1,0:T(2,128)(2,1)}), bf16[16,1,128]{2,1,0:T(2,128)(2,1)S(1)}, u32[]{:S(2)}, u32[]{:S(2)}) async-start(bf16[16,1,128]{2,1,0:T(2,128)(2,1)} %copy.61), calls=%async_computation.1 | async-start | bytes 16384 | tf_op jit(solution)/shard_map/all_to_all | solution.py:87
  31.0 0.7 fusion.70
  31.7 0.7 fusion.73
  32.4 0.8 convert_reduce_fusion
  33.6 1.1 fusion.88
  34.8 1.0 convolution_add_fusion
  35.8 1.6 fusion.13
  37.4 2.1 %fusion.6 = bf16[16,1,256]{2,0,1:T(8,128)(2,1)S(1)} fusion(bf16[4096,256]{1,0:T(8,128)(2,1)} %param.35, s32[16]{0:T(128)S(1)} %and_select_fusion.1, pred[16]{0:T(512)(128)(4,1)S(1)} %broadcast_compare_fusion.2, bf16[8,4096]{1,0:T(8,128)(2,1)S(1)} %all_gather.9, f32[4096]{0:T(1024)S(1)} %convert_element_type.145, f32[8]{0:T(128)S(1)} %add_rsqrt_fusion.2), kind=kOutput, calls=%fused_computation.16 | convolution fusion | flops 16980224 | bytes 2187376 | tf_op jit(solution)/shard_map/dot_general | solution.py:78
  39.9 0.8 dynamic-slice_convert_fusion
  41.3 0.6 reduce.5
  43.2 0.6 reduce.4
  44.5 6.0 %all-to-all-start = ((bf16[16,1,128]{2,1,0:T(2,128)(2,1)}), bf16[16,1,128]{2,1,0:T(2,128)(2,1)S(1)}, u32[]{:S(2)}, u32[]{:S(2)}) async-start(bf16[16,1,128]{2,1,0:T(2,128)(2,1)} %copy.59), calls=%async_computation | async-start | bytes 16384 | tf_op jit(solution)/shard_map/all_to_all | solution.py:86
  51.3 5.5 %all-to-all-done = bf16[16,1,128]{2,1,0:T(2,128)(2,1)S(1)} async-done(((bf16[16,1,128]{2,1,0:T(2,128)(2,1)}), bf16[16,1,128]{2,1,0:T(2,128)(2,1)S(1)}, u32[]{:S(2)}, u32[]{:S(2)}) %all-to-all-start) | async-done | bytes 4128 | tf_op jit(solution)/shard_map/all_to_all | solution.py:86
  56.8 3.4 %all-to-all-start.2 = ((bf16[16,2,128]{2,1,0:T(2,128)(2,1)}), bf16[16,2,128]{2,1,0:T(2,128)(2,1)S(1)}, u32[]{:S(2)}, u32[]{:S(2)}) async-start(bf16[16,2,128]{2,1,0:T(2,128)(2,1)} %reshape.330), calls=%async_computation.2 | async-start | bytes 16384 | tf_op jit(solution)/shard_map/all_to_all | solution.py:88
  61.1 5.6 %all-to-all-done.2 = bf16[16,2,128]{2,1,0:T(2,128)(2,1)S(1)} async-done(((bf16[16,2,128]{2,1,0:T(2,128)(2,1)}), bf16[16,2,128]{2,1,0:T(2,128)(2,1)S(1)}, u32[]{:S(2)}, u32[]{:S(2)}) %all-to-all-start.2) | async-done | bytes 8224 | tf_op jit(solution)/shard_map/all_to_all | solution.py:88
  66.6 3.5 %all-to-all-start.3 = ((bf16[16,2,128]{2,1,0:T(2,128)(2,1)}), bf16[16,2,128]{2,1,0:T(2,128)(2,1)S(1)}, u32[]{:S(2)}, u32[]{:S(2)}) async-start(bf16[16,2,128]{2,1,0:T(2,128)(2,1)} %reshape.328), calls=%async_computation.3 | async-start | bytes 16384 | tf_op jit(solution)/shard_map/all_to_all | solution.py:89
  71.0 2.7 %multiply_add_fusion = f32[2,512,1024]{2,1,0:T(8,128)S(1)} fusion(f32[2,512,1024]{2,1,0:T(8,128)} %param.30, f32[2,1024]{1,0:T(2,128)S(1)} %bitcast.122, f32[2,512]{1,0:T(2,128)S(1)} %bitcast.124, f32[2,512]{1,0:T(2,128)S(1)} %fusion.44), kind=kLoop, calls=%fused_computation.11 | loop fusion | flops 3145728 | bytes 8404992 | tf_op jit(solution)/shard_map/add | solution.py:116
  73.8 2.0 %copy-done.1 = f32[2,512,1024]{2,1,0:T(8,128)} copy-done((f32[2,512,1024]{2,1,0:T(8,128)}, f32[2,512,1024]{2,1,0:T(8,128)S(1)}, u32[]{:S(2)}) %copy-start.1) | copy-done | bytes 4194328
  75.8 2.1 %fusion.92 = f32[2,1,1024]{2,1,0:T(1,128)S(1)} fusion(f32[2,512,1]{1,2,0:T(1,128)S(1)} %bitcast.123, f32[2,512,1024]{2,1,0:T(8,128)S(1)} %multiply_add_fusion), kind=kOutput, calls=%fused_computation.142 | convolution fusion | flops 12582912 | bytes 4206592 | tf_op jit(solution)/shard_map/pk,pkv->pv/dot_general | solution.py:119
  78.9 21.8 %all-gather = bf16[16,2,1024]{2,1,0:T(2,128)(2,1)S(1)} all-gather(bf16[1,2,1024]{2,1,0:T(2,128)(2,1)S(1)} %fusion.60), channel_id=1, replica_groups=mesh['grp'=2,'ep'=16] {'ep'}, dimensions={0}, use_global_device_ids=true | all-gather | bytes 69632 | tf_op jit(solution)/shard_map/all_gather | solution.py:128
  100.8 2.1 %multiply_reduce_fusion = (f32[8]{0:T(128)S(1)}, f32[8,256]{1,0:T(8,128)S(1)}) fusion(bf16[8,4096]{1,0:T(8,128)(2,1)S(1)} %reshape.284, bf16[4096,256]{1,0:T(8,128)(2,1)} %param.40, bf16[8,256]{1,0:T(8,128)(2,1)S(1)} %copy-done.2), kind=kOutput, calls=%fused_computation.58 | convolution fusion | flops 16793592 | bytes 2175008 | tf_op jit(solution)/shard_map/dot_general | solution.py:129
  102.9 29.8 %psum.7 = f32[8]{0:T(128)S(1)} all-reduce(f32[8]{0:T(128)S(1)} %get-tuple-element.2), channel_id=1, replica_groups=mesh['grp'=2,'ep'=16] {'ep'}, use_global_device_ids=true, to_apply=%region_7.8 | all-reduce | flops 8 | bytes 64 | tf_op jit(solution)/shard_map/psum | solution.py:132
  132.8 17.3 %all_gather.11 = bf16[8,4096]{1,0:T(8,128)(2,1)S(1)} all-gather(bf16[8,256]{1,0:T(8,128)(2,1)S(1)} %multiply_convert_fusion), channel_id=1, replica_groups=mesh['grp'=2,'ep'=16] {'ep'}, dimensions={1}, use_global_device_ids=true | all-gather | bytes 69632 | tf_op jit(solution)/shard_map/all_gather | solution.py:135
  150.2 2.8 %fusion.3 = f32[2,512]{1,0:T(2,128)S(1)} fusion(bf16[2,4096]{1,0:T(2,128)(2,1)S(1)} %convolution_convert_fusion.1, bf16[1,4096,512]{2,1,0:T(8,128)(2,1)} %param.45), kind=kOutput, calls=%fused_computation.9 | convolution fusion | flops 8388608 | bytes 4214784 | tf_op jit(solution)/shard_map/dot_general | solution.py:149
  153.1 5.4 %convolution_convert_fusion = bf16[2,4096]{1,0:T(2,128)(2,1)} fusion(bf16[1,512,4096]{2,1,0:T(8,128)(2,1)} %param.47, bf16[2,4096]{1,0:T(2,128)(2,1)S(1)} %convolution_convert_fusion.1, bf16[1,4096,512]{2,1,0:T(8,128)(2,1)} %param.46, f32[2,512]{1,0:T(2,128)S(1)} %fusion.3, f32[2]{0:T(128)S(1)} %convolution_bitcast_fusion.5), kind=kOutput, calls=%fused_computation.4 | convolution fusion | flops 16792576 | bytes 8425480 | tf_op jit(solution)/shard_map/dot_general | solution.py:152
  158.4 3.5 %all-to-all-start.4 = ((bf16[2,16,256]{2,0,1:T(2,128)(2,1)}), bf16[2,16,256]{2,0,1:T(2,128)(2,1)S(1)}, u32[]{:S(2)}, u32[]{:S(2)}) async-start(bf16[2,16,256]{2,0,1:T(2,128)(2,1)} %bitcast.28), calls=%async_computation.4 | async-start | bytes 32768 | tf_op jit(solution)/shard_map/all_to_all | solution.py:155
  162.0 6.4 %all-to-all-done.4 = bf16[2,16,256]{2,0,1:T(2,128)(2,1)S(1)} async-done(((bf16[2,16,256]{2,0,1:T(2,128)(2,1)}), bf16[2,16,256]{2,0,1:T(2,128)(2,1)S(1)}, u32[]{:S(2)}, u32[]{:S(2)}) %all-to-all-start.4) | async-done | bytes 16416 | tf_op jit(solution)/shard_map/all_to_all | solution.py:155
  168.4 0.8 fusion.8
  (76 shorter events, 7.4 us)
Async XLA Ops:
  0.6 32.5 %copy-start = (bf16[4096,256]{1,0:T(8,128)(2,1)S(1)}, bf16[4096,256]{1,0:T(8,128)(2,1)}, u32[]{:S(2)}) copy-start(bf16[4096,256]{1,0:T(8,128)(2,1)} %param.34) | copy-start | bytes 6291460
  0.6 40.0 %copy-start.3 = (s32[8,2]{0,1:T(2,128)S(1)}, s32[8,2]{0,1:T(2,128)}, u32[]{:S(2)}) copy-start(s32[8,2]{0,1:T(2,128)} %param.42) | copy-start | bytes 196
  0.7 39.1 %copy-start.4 = (f32[8,4]{0,1:T(4,128)S(1)}, f32[8,4]{0,1:T(4,128)}, u32[]{:S(2)}) copy-start(f32[8,4]{0,1:T(4,128)} %param.43) | copy-start | bytes 388
  0.7 39.1 %copy-start.6 = (f32[8,2]{0,1:T(2,128)S(1)}, f32[8,2]{0,1:T(2,128)}, u32[]{:S(2)}) copy-start(f32[8,2]{0,1:T(2,128)} %param.44) | copy-start | bytes 196
  0.7 43.8 %copy-start.5 = (bf16[1024]{0:T(1024)(128)(2,1)S(1)}, bf16[1024]{0:T(1024)(128)(2,1)}, u32[]{:S(2)}) copy-start(bf16[1024]{0:T(1024)(128)(2,1)} %param.39) | copy-start | bytes 6148
  27.5 16.9 %all-to-all-start.1 = ((bf16[16,1,128]{2,1,0:T(2,128)(2,1)}), bf16[16,1,128]{2,1,0:T(2,128)(2,1)S(1)}, u32[]{:S(2)}, u32[]{:S(2)}) async-start(bf16[16,1,128]{2,1,0:T(2,128)(2,1)} %copy.61), calls=%async_computation.1 | async-start | bytes 16384 | tf_op jit(solution)/shard_map/all_to_all | solution.py:87
  44.5 12.3 %all-to-all-start = ((bf16[16,1,128]{2,1,0:T(2,128)(2,1)}), bf16[16,1,128]{2,1,0:T(2,128)(2,1)S(1)}, u32[]{:S(2)}, u32[]{:S(2)}) async-start(bf16[16,1,128]{2,1,0:T(2,128)(2,1)} %copy.59), calls=%async_computation | async-start | bytes 16384 | tf_op jit(solution)/shard_map/all_to_all | solution.py:86
  56.8 9.8 %all-to-all-start.2 = ((bf16[16,2,128]{2,1,0:T(2,128)(2,1)}), bf16[16,2,128]{2,1,0:T(2,128)(2,1)S(1)}, u32[]{:S(2)}, u32[]{:S(2)}) async-start(bf16[16,2,128]{2,1,0:T(2,128)(2,1)} %reshape.330), calls=%async_computation.2 | async-start | bytes 16384 | tf_op jit(solution)/shard_map/all_to_all | solution.py:88
  66.6 11.3 %all-to-all-start.3 = ((bf16[16,2,128]{2,1,0:T(2,128)(2,1)}), bf16[16,2,128]{2,1,0:T(2,128)(2,1)S(1)}, u32[]{:S(2)}, u32[]{:S(2)}) async-start(bf16[16,2,128]{2,1,0:T(2,128)(2,1)} %reshape.328), calls=%async_computation.3 | async-start | bytes 16384 | tf_op jit(solution)/shard_map/all_to_all | solution.py:89
  73.7 2.0 %copy-start.1 = (f32[2,512,1024]{2,1,0:T(8,128)}, f32[2,512,1024]{2,1,0:T(8,128)S(1)}, u32[]{:S(2)}) copy-start(f32[2,512,1024]{2,1,0:T(8,128)S(1)} %multiply_add_fusion) | copy-start | bytes 12582916
  73.8 27.0 %copy-start.2 = (bf16[8,256]{1,0:T(8,128)(2,1)S(1)}, bf16[8,256]{1,0:T(8,128)(2,1)}, u32[]{:S(2)}) copy-start(bf16[8,256]{1,0:T(8,128)(2,1)} %param.29) | copy-start | bytes 12292
  158.4 10.0 %all-to-all-start.4 = ((bf16[2,16,256]{2,0,1:T(2,128)(2,1)}), bf16[2,16,256]{2,0,1:T(2,128)(2,1)S(1)}, u32[]{:S(2)}, u32[]{:S(2)}) async-start(bf16[2,16,256]{2,0,1:T(2,128)(2,1)} %bitcast.28), calls=%async_computation.4 | async-start | bytes 32768 | tf_op jit(solution)/shard_map/all_to_all | solution.py:155
where the time goes:
time: 170 us; the launch traced here: 169 us
  blocking collectives  92.6 us (54%)
  matrix products  22.2 us (13%)
  starting transfers between devices  19.8 us (12%)
  waiting for transfers between devices  17.5 us (10%)
  other arithmetic  8.69 us (5%)
  local copies, waits for them, and re-layouts  7.43 us (4%)
    psum x1, blocking collectives, per_device(): total = lax.psum(jnp.sum(floats * floats, axis=1), 'ep')  29.8 us
    all_gather x1, blocking collectives, per_device(): rows = lax.all_gather(residual, 'ep', axis=1, tiled=True)  23.7 us
    all_gather x1, blocking collectives, per_device(): lax.all_gather(mixed, 'ep', axis=0, tiled=True)  21.8 us
    all_gather x1, blocking collectives, per_device(): lax.all_gather(scaled.astype(jnp.bfloat16), 'ep', axis=1, tiled=True)  17.3 us
    all_to_all x1, waiting for transfers between devices, per_device(): lax.all_to_all(expert_rows, 'ep', split_axis=1, concat_axis=0, tiled=True)  6.42 us
    all_to_all x1, starting transfers between devices, per_device(): lax.all_to_all(send_query, 'ep', split_axis=0, concat_axis=0, tiled=True)  5.98 us
    dot_general x4, matrix products, outgoing(): jnp.dot(picker, projected, preferred_element_type=jnp.float32)  5.92 us
    all_to_all x1, waiting for transfers between devices, per_device(): lax.all_to_all(send_value, 'ep', split_axis=0, concat_axis=0, tiled=True)  5.56 us
  transfers between devices with their start and end apart: 5, of which 3 were waited for; matrix products, arithmetic and copies ran while one was open for 12% of the time, Pallas kernels for 0%

commit v1 on v0

--- a/solution.py
+++ b/solution.py
@@ -62,7 +62,7 @@
     width = own_width * devices
     pairs_dev = head_states.shape[0]
     slot_count = max(1, pairs_dev // HEADS)
-    rows = lax.all_gather(residual, "ep", axis=1, tiled=True)
+    rows = jnp.concatenate(lax.all_gather(residual, "ep"), axis=1)
     normed = rms_scale(rows, first_gain).astype(jnp.bfloat16)
     my_head = my_index * HEADS // devices
     target = jnp.arange(devices, dtype=jnp.int32)[:, None]

time: 170 us -> 168 us (0.988)
  no operation moved by 1% of the time
where the time goes in v1:
time: 168 us
  blocking collectives  92.6 us (55%)
  matrix products  20.6 us (12%)
  starting transfers between devices  19.8 us (12%)
  waiting for transfers between devices  17.5 us (10%)
  other arithmetic  8.78 us (5%)
  local copies, waits for them, and re-layouts  7.44 us (4%)
    psum x1, blocking collectives, per_device(): total = lax.psum(jnp.sum(floats * floats, axis=1), 'ep')  29.8 us
    all_gather x1, blocking collectives, per_device(): rows = jnp.concatenate(lax.all_gather(residual, 'ep'), axis=1)  23.7 us
    all_gather x1, blocking collectives, per_device(): lax.all_gather(mixed, 'ep', axis=0, tiled=True)  21.8 us
    all_gather x1, blocking collectives, per_device(): lax.all_gather(scaled.astype(jnp.bfloat16), 'ep', axis=1, tiled=True)  17.3 us
    all_to_all x1, waiting for transfers between devices, per_device(): lax.all_to_all(expert_rows, 'ep', split_axis=1, concat_axis=0, tiled=True)  6.42 us
    all_to_all x1, starting transfers between devices, per_device(): lax.all_to_all(send_query, 'ep', split_axis=0, concat_axis=0, tiled=True)  5.98 us
    all_to_all x1, waiting for transfers between devices, per_device(): lax.all_to_all(send_value, 'ep', split_axis=0, concat_axis=0, tiled=True)  5.56 us
    all_to_all x1, waiting for transfers between devices, per_device(): lax.all_to_all(send_query, 'ep', split_axis=0, concat_axis=0, tiled=True)  5.53 us
  transfers between devices with their start and end apart: 5, of which 3 were waited for; matrix products, arithmetic and copies ran while one was open for 12% of the time, Pallas kernels for 0%

profile of v1, /device:TPU:0, one launch (start us, length us, event | category | flops | bytes accessed | tf_op | source)
XLA Modules:
  0.0 167.7 jit_solution(15375977414009052667)
XLA Ops:
  0.8 23.7 %all-gather = bf16[128,256]{1,0:T(8,128)(2,1)S(1)} all-gather(bf16[8,256]{1,0:T(8,128)(2,1)} %param.29), channel_id=2, replica_groups=mesh['grp'=2,'ep'=16] {'ep'}, dimensions={0}, use_global_device_ids=true | all-gather | bytes 69632 | tf_op jit(solution)/shard_map/all_gather | solution.py:65
  24.6 0.7 convert_element_type.158
  25.4 1.6 fusion.14
  27.0 0.6 copy.61
  27.6 3.4 %all-to-all-start.1 = ((bf16[16,1,128]{2,1,0:T(2,128)(2,1)}), bf16[16,1,128]{2,1,0:T(2,128)(2,1)S(1)}, u32[]{:S(2)}, u32[]{:S(2)}) async-start(bf16[16,1,128]{2,1,0:T(2,128)(2,1)} %copy.61), calls=%async_computation.1 | async-start | bytes 16384 | tf_op jit(solution)/shard_map/all_to_all | solution.py:87
  31.0 0.7 fusion.67
  31.7 0.7 fusion.70
  32.4 0.8 convert_reduce_fusion
  33.7 1.1 fusion.79
  34.7 0.9 convolution_add_fusion
  36.0 2.1 %fusion.6 = bf16[16,1,256]{2,0,1:T(8,128)(2,1)S(1)} fusion(bf16[8,4096]{1,0:T(8,128)(2,1)S(1)} %multiply_convert_fusion, bf16[4096,256]{1,0:T(8,128)(2,1)} %param.35, s32[16]{0:T(128)S(1)} %and_select_fusion.1, pred[16]{0:T(512)(128)(4,1)S(1)} %broadcast_compare_fusion.2), kind=kOutput, calls=%fused_computation.16 | convolution fusion | flops 16849152 | bytes 2170960 | tf_op jit(solution)/shard_map/dot_general | solution.py:78
  38.4 0.8 dynamic-slice_convert_fusion
  39.9 0.6 reduce.7
  41.7 0.6 reduce.6
  42.4 0.6 reshape.336
  43.0 6.0 %all-to-all-start = ((bf16[16,1,128]{2,1,0:T(2,128)(2,1)}), bf16[16,1,128]{2,1,0:T(2,128)(2,1)S(1)}, u32[]{:S(2)}, u32[]{:S(2)}) async-start(bf16[16,1,128]{2,1,0:T(2,128)(2,1)} %copy.59), calls=%async_computation | async-start | bytes 16384 | tf_op jit(solution)/shard_map/all_to_all | solution.py:86
  49.8 5.5 %all-to-all-done = bf16[16,1,128]{2,1,0:T(2,128)(2,1)S(1)} async-done(((bf16[16,1,128]{2,1,0:T(2,128)(2,1)}), bf16[16,1,128]{2,1,0:T(2,128)(2,1)S(1)}, u32[]{:S(2)}, u32[]{:S(2)}) %all-to-all-start) | async-done | bytes 4128 | tf_op jit(solution)/shard_map/all_to_all | solution.py:86
  55.4 3.4 %all-to-all-start.2 = ((bf16[16,2,128]{2,1,0:T(2,128)(2,1)}), bf16[16,2,128]{2,1,0:T(2,128)(2,1)S(1)}, u32[]{:S(2)}, u32[]{:S(2)}) async-start(bf16[16,2,128]{2,1,0:T(2,128)(2,1)} %reshape.338), calls=%async_computation.2 | async-start | bytes 16384 | tf_op jit(solution)/shard_map/all_to_all | solution.py:88
  59.6 5.6 %all-to-all-done.2 = bf16[16,2,128]{2,1,0:T(2,128)(2,1)S(1)} async-done(((bf16[16,2,128]{2,1,0:T(2,128)(2,1)}), bf16[16,2,128]{2,1,0:T(2,128)(2,1)S(1)}, u32[]{:S(2)}, u32[]{:S(2)}) %all-to-all-start.2) | async-done | bytes 8224 | tf_op jit(solution)/shard_map/all_to_all | solution.py:88
  65.2 3.5 %all-to-all-start.3 = ((bf16[16,2,128]{2,1,0:T(2,128)(2,1)}), bf16[16,2,128]{2,1,0:T(2,128)(2,1)S(1)}, u32[]{:S(2)}, u32[]{:S(2)}) async-start(bf16[16,2,128]{2,1,0:T(2,128)(2,1)} %reshape.336), calls=%async_computation.3 | async-start | bytes 16384 | tf_op jit(solution)/shard_map/all_to_all | solution.py:89
  69.5 2.7 %multiply_add_fusion = f32[2,512,1024]{2,1,0:T(8,128)S(1)} fusion(f32[2,512,1024]{2,1,0:T(8,128)} %param.30, f32[2,1024]{1,0:T(2,128)S(1)} %bitcast.136, f32[2,512]{1,0:T(2,128)S(1)} %bitcast.138, f32[2,512]{1,0:T(2,128)S(1)} %fusion.41), kind=kLoop, calls=%fused_computation.11 | loop fusion | flops 3145728 | bytes 8404992 | tf_op jit(solution)/shard_map/add | solution.py:116
  72.3 2.0 %copy-done.1 = f32[2,512,1024]{2,1,0:T(8,128)} copy-done((f32[2,512,1024]{2,1,0:T(8,128)}, f32[2,512,1024]{2,1,0:T(8,128)S(1)}, u32[]{:S(2)}) %copy-start.1) | copy-done | bytes 4194328
  74.3 2.1 %fusion.80 = f32[2,1,1024]{2,1,0:T(1,128)S(1)} fusion(f32[2,512,1]{1,2,0:T(1,128)S(1)} %bitcast.137, f32[2,512,1024]{2,1,0:T(8,128)S(1)} %multiply_add_fusion), kind=kOutput, calls=%fused_computation.140 | convolution fusion | flops 12582912 | bytes 4206592 | tf_op jit(solution)/shard_map/pk,pkv->pv/dot_general | solution.py:119
  77.5 21.8 %all-gather.1 = bf16[16,2,1024]{2,1,0:T(2,128)(2,1)S(1)} all-gather(bf16[1,2,1024]{2,1,0:T(2,128)(2,1)S(1)} %fusion.57), channel_id=1, replica_groups=mesh['grp'=2,'ep'=16] {'ep'}, dimensions={0}, use_global_device_ids=true | all-gather | bytes 69632 | tf_op jit(solution)/shard_map/all_gather | solution.py:128
  99.3 2.1 %multiply_reduce_fusion.1 = (f32[8]{0:T(128)S(1)}, f32[8,256]{1,0:T(8,128)S(1)}) fusion(bf16[8,4096]{1,0:T(8,128)(2,1)S(1)} %reshape.288, bf16[4096,256]{1,0:T(8,128)(2,1)} %param.40, bf16[8,256]{1,0:T(8,128)(2,1)S(1)} %copy-done.4), kind=kOutput, calls=%fused_computation.56 | convolution fusion | flops 16793592 | bytes 2175008 | tf_op jit(solution)/shard_map/dot_general | solution.py:129
  101.4 29.8 %psum.7 = f32[8]{0:T(128)S(1)} all-reduce(f32[8]{0:T(128)S(1)} %get-tuple-element.2), channel_id=1, replica_groups=mesh['grp'=2,'ep'=16] {'ep'}, use_global_device_ids=true, to_apply=%region_7.8 | all-reduce | flops 8 | bytes 64 | tf_op jit(solution)/shard_map/psum | solution.py:132
  131.3 17.3 %all_gather.15 = bf16[8,4096]{1,0:T(8,128)(2,1)S(1)} all-gather(bf16[8,256]{1,0:T(8,128)(2,1)S(1)} %multiply_convert_fusion.1), channel_id=1, replica_groups=mesh['grp'=2,'ep'=16] {'ep'}, dimensions={1}, use_global_device_ids=true | all-gather | bytes 69632 | tf_op jit(solution)/shard_map/all_gather | solution.py:135
  148.8 2.8 %fusion.3 = f32[2,512]{1,0:T(2,128)S(1)} fusion(bf16[2,4096]{1,0:T(2,128)(2,1)S(1)} %convolution_convert_fusion.1, bf16[1,4096,512]{2,1,0:T(8,128)(2,1)} %param.45), kind=kOutput, calls=%fused_computation.9 | convolution fusion | flops 8388608 | bytes 4214784 | tf_op jit(solution)/shard_map/dot_general | solution.py:149
  151.6 5.4 %convolution_convert_fusion = bf16[2,4096]{1,0:T(2,128)(2,1)} fusion(bf16[1,512,4096]{2,1,0:T(8,128)(2,1)} %param.47, bf16[2,4096]{1,0:T(2,128)(2,1)S(1)} %convolution_convert_fusion.1, bf16[1,4096,512]{2,1,0:T(8,128)(2,1)} %param.46, f32[2,512]{1,0:T(2,128)S(1)} %fusion.3, f32[2]{0:T(128)S(1)} %convolution_bitcast_fusion.5), kind=kOutput, calls=%fused_computation.4 | convolution fusion | flops 16792576 | bytes 8425480 | tf_op jit(solution)/shard_map/dot_general | solution.py:152
  156.9 3.5 %all-to-all-start.4 = ((bf16[2,16,256]{2,0,1:T(2,128)(2,1)}), bf16[2,16,256]{2,0,1:T(2,128)(2,1)S(1)}, u32[]{:S(2)}, u32[]{:S(2)}) async-start(bf16[2,16,256]{2,0,1:T(2,128)(2,1)} %bitcast.32), calls=%async_computation.4 | async-start | bytes 32768 | tf_op jit(solution)/shard_map/all_to_all | solution.py:155
  160.5 6.4 %all-to-all-done.4 = bf16[2,16,256]{2,0,1:T(2,128)(2,1)S(1)} async-done(((bf16[2,16,256]{2,0,1:T(2,128)(2,1)}), bf16[2,16,256]{2,0,1:T(2,128)(2,1)S(1)}, u32[]{:S(2)}, u32[]{:S(2)}) %all-to-all-start.4) | async-done | bytes 16416 | tf_op jit(solution)/shard_map/all_to_all | solution.py:155
  166.9 0.8 fusion.8
  (82 shorter events, 7.2 us)
Async XLA Ops:
  0.6 32.6 %copy-start = (bf16[4096,256]{1,0:T(8,128)(2,1)S(1)}, bf16[4096,256]{1,0:T(8,128)(2,1)}, u32[]{:S(2)}) copy-start(bf16[4096,256]{1,0:T(8,128)(2,1)} %param.34) | copy-start | bytes 6291460
  0.6 38.5 %copy-start.5 = (s32[8,2]{0,1:T(2,128)S(1)}, s32[8,2]{0,1:T(2,128)}, u32[]{:S(2)}) copy-start(s32[8,2]{0,1:T(2,128)} %param.42) | copy-start | bytes 196
  0.7 34.1 %copy-start.3 = (bf16[16,2048]{1,0:T(8,128)(2,1)S(1)}, bf16[16,2048]{1,0:T(8,128)(2,1)}, u32[]{:S(2)}) copy-start(bf16[16,2048]{1,0:T(8,128)(2,1)} %param.37) | copy-start | bytes 196612
  0.7 35.0 %copy-start.2 = (bf16[4096,128]{1,0:T(8,128)(2,1)S(1)}, bf16[4096,128]{1,0:T(8,128)(2,1)}, u32[]{:S(2)}) copy-start(bf16[4096,128]{1,0:T(8,128)(2,1)} %param.32) | copy-start | bytes 3145732
  0.7 37.6 %copy-start.6 = (f32[8,4]{0,1:T(4,128)S(1)}, f32[8,4]{0,1:T(4,128)}, u32[]{:S(2)}) copy-start(f32[8,4]{0,1:T(4,128)} %param.43) | copy-start | bytes 388
  0.7 37.6 %copy-start.8 = (f32[8,2]{0,1:T(2,128)S(1)}, f32[8,2]{0,1:T(2,128)}, u32[]{:S(2)}) copy-start(f32[8,2]{0,1:T(2,128)} %param.44) | copy-start | bytes 196
  0.7 42.3 %copy-start.7 = (bf16[1024]{0:T(1024)(128)(2,1)S(1)}, bf16[1024]{0:T(1024)(128)(2,1)}, u32[]{:S(2)}) copy-start(bf16[1024]{0:T(1024)(128)(2,1)} %param.39) | copy-start | bytes 6148
  27.6 15.4 %all-to-all-start.1 = ((bf16[16,1,128]{2,1,0:T(2,128)(2,1)}), bf16[16,1,128]{2,1,0:T(2,128)(2,1)S(1)}, u32[]{:S(2)}, u32[]{:S(2)}) async-start(bf16[16,1,128]{2,1,0:T(2,128)(2,1)} %copy.61), calls=%async_computation.1 | async-start | bytes 16384 | tf_op jit(solution)/shard_map/all_to_all | solution.py:87
  43.0 12.3 %all-to-all-start = ((bf16[16,1,128]{2,1,0:T(2,128)(2,1)}), bf16[16,1,128]{2,1,0:T(2,128)(2,1)S(1)}, u32[]{:S(2)}, u32[]{:S(2)}) async-start(bf16[16,1,128]{2,1,0:T(2,128)(2,1)} %copy.59), calls=%async_computation | async-start | bytes 16384 | tf_op jit(solution)/shard_map/all_to_all | solution.py:86
  55.4 9.8 %all-to-all-start.2 = ((bf16[16,2,128]{2,1,0:T(2,128)(2,1)}), bf16[16,2,128]{2,1,0:T(2,128)(2,1)S(1)}, u32[]{:S(2)}, u32[]{:S(2)}) async-start(bf16[16,2,128]{2,1,0:T(2,128)(2,1)} %reshape.338), calls=%async_computation.2 | async-start | bytes 16384 | tf_op jit(solution)/shard_map/all_to_all | solution.py:88
  65.2 11.3 %all-to-all-start.3 = ((bf16[16,2,128]{2,1,0:T(2,128)(2,1)}), bf16[16,2,128]{2,1,0:T(2,128)(2,1)S(1)}, u32[]{:S(2)}, u32[]{:S(2)}) async-start(bf16[16,2,128]{2,1,0:T(2,128)(2,1)} %reshape.336), calls=%async_computation.3 | async-start | bytes 16384 | tf_op jit(solution)/shard_map/all_to_all | solution.py:89
  72.3 2.0 %copy-start.1 = (f32[2,512,1024]{2,1,0:T(8,128)}, f32[2,512,1024]{2,1,0:T(8,128)S(1)}, u32[]{:S(2)}) copy-start(f32[2,512,1024]{2,1,0:T(8,128)S(1)} %multiply_add_fusion) | copy-start | bytes 12582916
  72.3 27.0 %copy-start.4 = (bf16[8,256]{1,0:T(8,128)(2,1)S(1)}, bf16[8,256]{1,0:T(8,128)(2,1)}, u32[]{:S(2)}) copy-start(bf16[8,256]{1,0:T(8,128)(2,1)} %param.29) | copy-start | bytes 12292
  156.9 10.0 %all-to-all-start.4 = ((bf16[2,16,256]{2,0,1:T(2,128)(2,1)}), bf16[2,16,256]{2,0,1:T(2,128)(2,1)S(1)}, u32[]{:S(2)}, u32[]{:S(2)}) async-start(bf16[2,16,256]{2,0,1:T(2,128)(2,1)} %bitcast.32), calls=%async_computation.4 | async-start | bytes 32768 | tf_op jit(solution)/shard_map/all_to_all | solution.py:155
